TPU v7x, 32 devices: a whole 2x2x4 slice. The times are simulated.
32 devices in a mesh: ep: 8 (over z, core), tp: 4 (over y, x).
Axes of the slice: x: 2, y: 2, z: 4, core: 2. Of those that a mesh axis runs over, the one named last changes fastest.
Arguments:
- mix_rows: bfloat16 [2048, 2048], P('ep', 'tp'), may hold values from -6 to 6
- mix_gain: bfloat16 [2048], replicated, may hold values from 0.099609375 to 1.8984375
- w_query: bfloat16 [2048, 2048], P(None, 'tp'), may hold values from -0.125 to 0.125
- w_forget: bfloat16 [2048, 2048], P(None, 'tp'), may hold values from -0.125 to 0.125
- w_input: bfloat16 [2048, 2048], P(None, 'tp'), may hold values from -0.125 to 0.125
- w_outgate: bfloat16 [2048, 2048], P(None, 'tp'), may hold values from -0.125 to 0.125
- forget_gap: float32 [2048], P('tp'), may hold values from 1e-05 to 0.1
- decay_extra: float32 [16, 2048], P('tp', 'ep'), may hold values from -0.7 to 0, as said below
- head_gain: bfloat16 [128], replicated, may hold values from 0.099609375 to 1.8984375
- w_mixout: bfloat16 [2048, 2048], P('tp'), may hold values from -0.125 to 0.125
- moe_rows: bfloat16 [2048, 2048], P('ep', 'tp'), may hold values from -6 to 6
- moe_gain: bfloat16 [2048], replicated, may hold values from 0.099609375 to 1.8984375
- route_ids: int32 [2048, 2], P('ep'), may hold values from 0 to 7, all different within a row; in each aligned block of 256 rows (0 to 255, 256 to 511, ...) at most 96 rows name the same one
- route_scores: float32 [2048, 2], P('ep'), may hold values from 0.05 to 1
- w_gate: bfloat16 [8, 2048, 3072], P('ep', None, 'tp'), may hold values from -0.125 to 0.125
- w_up: bfloat16 [8, 2048, 3072], P('ep', None, 'tp'), may hold values from -0.125 to 0.125
- w_down: bfloat16 [8, 3072, 2048], P('ep', 'tp'), may hold values from -0.109375 to 0.109375
Outputs:
- mix_out: bfloat16 [2048, 2048], P('ep', 'tp')
- moe_out: bfloat16 [2048, 2048], P('ep', 'tp')
Inputs may be any that keep to these rules, and one draw needn't show every extreme that they name: `route_ids`: each row names 2 different experts. Among the rows of one index of ep at most 96 name the same expert, a bound that at least one block reaches. `decay_extra`: never positive.
All inputs are finite; a program needn't handle non-finite values.
Results may differ from a plain program's by a relative error of at most 0.017.
Values may be sent and summed in bfloat16 or wider, within the bound.
A program may use at most 64 MiB of HBM per device.

v0:
```python
import jax
import jax.numpy as jnp
from jax import lax
from jax.sharding import PartitionSpec as P

BLOCK = 64


epsilon = 1e-06
HIGHEST_PRECISION = lax.Precision.HIGHEST


def entering(x, axis, join, neutral):
    place = lax.axis_index(axis)
    gathered = jax.tree.map(
        lambda a, kind: lax.all_gather(a.astype(kind), axis), x, (jnp.bfloat16, jnp.bfloat16)
    )
    state = jax.tree.map(lambda a, e: jnp.zeros_like(a) + jnp.asarray(e, a.dtype), x, neutral)

    def one(hop, state):
        return join(
            state,
            jax.tree.map(
                lambda a, own: lax.dynamic_index_in_dim(a, hop, 0, False).astype(own.dtype),
                gathered,
                x,
            ),
        )

    return lax.fori_loop(0, place, one, state)


def rms_scale(rows, gain):
    values = rows.astype(jnp.float32)
    scale = lax.rsqrt(jnp.mean(values * values, axis=-1, keepdims=True) + epsilon)
    return values * scale * gain.astype(jnp.float32)


def block_recurrence(query_rows, key_in, value, log_forget, state):
    heads_count, length, key_dim = query_rows.shape
    block_list = length // BLOCK

    def split(values):
        return jnp.moveaxis(values.reshape(heads_count, block_list, BLOCK, values.shape[2]), 1, 0)

    causal = jnp.tril(jnp.ones((BLOCK, BLOCK), dtype=bool))[:, :, None]

    def advance(carry, inputs):
        query_block, key_block, value_block, forget_block = inputs
        running_state = jnp.cumsum(forget_block, axis=1)
        spread = running_state[:, :, None, :] - running_state[:, None, :, :]
        decay = jnp.exp(jnp.where(causal, spread, -jnp.inf))
        scores = jnp.einsum(
            "hid,hjd,hijd->hij", query_block, key_block, decay, precision=HIGHEST_PRECISION
        )
        output = jnp.einsum(
            "hid,hde->hie", query_block * jnp.exp(running_state), carry, precision=HIGHEST_PRECISION
        )
        output = output + jnp.einsum(
            "hij,hje->hie", scores, value_block, precision=HIGHEST_PRECISION
        )
        last = running_state[:, -1:, :]
        carry = carry * jnp.exp(last)[:, 0, :, None] + jnp.einsum(
            "hjd,hje->hde",
            key_block * jnp.exp(last - running_state),
            value_block,
            precision=HIGHEST_PRECISION,
        )
        return (carry, output)

    carry, outputs = lax.scan(
        advance, state, (split(query_rows), split(key_in), split(value), split(log_forget))
    )
    return (jnp.moveaxis(outputs, 0, 1).reshape(heads_count, length, value.shape[2]), carry)


def chain(earlier, later):
    return (earlier[0] * later[0], later[0][:, :, None] * earlier[1] + later[1])


def per_device(
    mix_rows,
    mix_gain,
    w_query,
    w_forget,
    w_input,
    w_outgate,
    forget_gap,
    decay_extra,
    head_gain,
    w_mixout,
    moe_rows,
    moe_gain,
    route_ids,
    route_scores,
    w_gate,
    w_up,
    w_down,
):
    col_width = mix_rows.shape[1]
    ep_count = lax.axis_size("ep")
    model_width = col_width * lax.axis_size("tp")
    mix_whole = lax.all_gather(mix_rows, "tp", axis=1, tiled=True)
    moe_values = moe_rows.astype(jnp.float32)
    squares = lax.psum(jnp.sum(moe_values * moe_values, axis=1), "tp")
    gain_cols = lax.dynamic_slice_in_dim(moe_gain, lax.axis_index("tp") * col_width, col_width, 0)
    expert_scale = lax.rsqrt(squares / model_width + epsilon)[:, None]
    moe_normed = (moe_values * expert_scale * gain_cols.astype(jnp.float32)).astype(jnp.bfloat16)
    mix_normed = rms_scale(mix_whole, mix_gain).astype(jnp.bfloat16)
    length = mix_normed.shape[0]
    heads_dev = decay_extra.shape[0]

    def heads(values):
        return values.reshape(length, heads_dev, -1).transpose(1, 0, 2)

    query_preactivation = jnp.dot(mix_normed, w_query, preferred_element_type=jnp.float32)
    forget_pre = jnp.dot(mix_normed, w_forget, preferred_element_type=jnp.float32)
    input_pre = jnp.dot(mix_normed, w_input, preferred_element_type=jnp.float32)
    outgate_pre = jnp.dot(mix_normed, w_outgate, preferred_element_type=jnp.float32)
    query_rows = heads(jax.nn.silu(query_preactivation))
    key_in = heads(forget_gap * jax.nn.sigmoid(-forget_pre))
    value = heads(input_pre)
    log_forget = jnp.log1p(-key_in) + decay_extra[:, :, None]
    start_state = jnp.zeros((heads_dev, query_rows.shape[2], value.shape[2]), jnp.float32)
    local_out, local_state = block_recurrence(query_rows, key_in, value, log_forget, start_state)
    running_state = jnp.cumsum(log_forget, axis=1)
    passing = jnp.exp(running_state[:, -1, :])
    carried_state = entering(
        (passing, local_state), "ep", chain, (jnp.ones_like(passing), jnp.zeros_like(local_state))
    )[1]
    head_out = local_out + jnp.einsum(
        "won,wnd->wod",
        query_rows * jnp.exp(running_state),
        carried_state,
        precision=HIGHEST_PRECISION,
    )
    gated = rms_scale(head_out, head_gain) * heads(jax.nn.silu(outgate_pre))
    gated = gated.transpose(1, 0, 2).reshape(length, -1).astype(jnp.bfloat16)
    piece = w_mixout
    mix_sum = lax.psum_scatter(
        lax.dot_general(
            piece, gated, (((0,), (1,)), ((), ())), preferred_element_type=jnp.float32
        ).astype(jnp.bfloat16),
        "tp",
        scatter_dimension=0,
        tiled=True,
    )
    mix_out = mix_sum.T
    tok_count, top_count = route_ids.shape
    local_experts = w_gate.shape[0]
    expert_count = local_experts * ep_count
    capacity = tok_count * top_count * 3 // (2 * expert_count)
    weights = route_scores / jnp.sum(route_scores, axis=1, keepdims=True)
    chosen = route_ids.reshape(-1)
    onehot = (chosen[:, None] == jnp.arange(expert_count, dtype=jnp.int32)[None, :]).astype(
        jnp.int32
    )
    rank = jnp.sum((jnp.cumsum(onehot, axis=0) - 1) * onehot, axis=1)
    place = chosen * capacity + rank
    token = jnp.arange(tok_count * top_count, dtype=jnp.int32) // top_count
    table = jnp.full((expert_count * capacity,), tok_count, jnp.int32).at[place].set(token)
    padded = jnp.concatenate(
        [moe_normed, jnp.zeros((1, moe_normed.shape[1]), jnp.bfloat16)], axis=0
    )
    slots = padded[table].reshape(ep_count, local_experts, capacity, -1)
    arrived = lax.all_to_all(slots, "ep", split_axis=0, concat_axis=0, tiled=True)
    piece = lax.all_gather(arrived, "tp", axis=3, tiled=True)
    gate_acts = jnp.einsum("secd,edf->secf", piece, w_gate, preferred_element_type=jnp.float32)
    up_acts = jnp.einsum("secd,edf->secf", piece, w_up, preferred_element_type=jnp.float32)
    hidden = (jax.nn.silu(gate_acts) * up_acts).astype(jnp.bfloat16)
    piece = w_down
    product = jnp.einsum("secf,efo->osec", hidden, piece, preferred_element_type=jnp.float32)
    expert_sum = lax.psum_scatter(
        product.reshape(col_width * lax.axis_size("tp"), -1).astype(jnp.bfloat16),
        "tp",
        scatter_dimension=0,
        tiled=True,
    )
    outgoing = expert_sum.reshape(col_width, ep_count, -1)
    returned = lax.all_to_all(outgoing, "ep", split_axis=1, concat_axis=1, tiled=True)
    picked = jnp.take(returned.reshape(col_width, -1), place, axis=1).astype(jnp.float32)
    picked = picked.reshape(col_width, tok_count, top_count)
    moe_out = jnp.sum(picked * weights[None, :, :], axis=2).T.astype(jnp.bfloat16)
    return (mix_out, moe_out)


def solution(mesh):
    placed = (
        P("ep", "tp"),
        P(),
        P(None, "tp"),
        P(None, "tp"),
        P(None, "tp"),
        P(None, "tp"),
        P("tp"),
        P("tp", "ep"),
        P(),
        P("tp", None),
        P("ep", "tp"),
        P(),
        P("ep", None),
        P("ep", None),
        P("ep", None, "tp"),
        P("ep", None, "tp"),
        P("ep", "tp", None),
    )
    return jax.shard_map(
        per_device,
        mesh=mesh,
        in_specs=placed,
        out_specs=(P("ep", "tp"), P("ep", "tp")),
        check_vma=False,
    )
```

profile of v0, /device:TPU:0, one launch (start us, length us, event | category | flops | bytes accessed | tf_op | source)
XLA Modules:
  0.0 251.6 jit_solution(13833511479303720452)
XLA Ops:
  11.0 11.4 %psum.7 = f32[256]{0:T(256)S(1)} all-reduce(f32[256]{0:T(256)S(1)} %fusion.50), channel_id=1, replica_groups=mesh['ep'=8,'tp'=4] {'tp'}, use_global_device_ids=true, to_apply=%region_14.15 | all-reduce | flops 256 | bytes 2048 | tf_op jit(solution)/shard_map/psum | solution.py:105
  26.7 2.4 scatter_custom_fusion
  30.2 3.3 %gather_fusion = bf16[768,512]{1,0:T(8,128)(2,1)} fusion(bf16[257,512]{1,0:T(8,128)(2,1)S(1)} %concatenate.3, s32[1024]{0:T(1024)S(1)} %pad_clamp_fusion.1), kind=kCustom, calls=%fused_computation | custom fusion | bytes 1575936 | tf_op jit(solution)/shard_map/gather | solution.py:165
  33.5 5.0 %all-to-all-start = ((bf16[8,1,96,512]{3,2,1,0:T(8,128)(2,1)}), bf16[8,1,96,512]{3,2,1,0:T(8,128)(2,1)}, u32[]{:S(2)}, u32[]{:S(2)}) async-start(bf16[8,1,96,512]{3,2,1,0:T(8,128)(2,1)} %bitcast.234), calls=%async_computation.1 | async-start | bytes 1572864 | tf_op jit(solution)/shard_map/all_to_all | solution.py:166
  38.6 21.0 %all-to-all-done = bf16[8,1,96,512]{3,2,1,0:T(8,128)(2,1)} async-done(((bf16[8,1,96,512]{3,2,1,0:T(8,128)(2,1)}), bf16[8,1,96,512]{3,2,1,0:T(8,128)(2,1)}, u32[]{:S(2)}, u32[]{:S(2)}) %all-to-all-start) | async-done | bytes 786464 | tf_op jit(solution)/shard_map/all_to_all | solution.py:166
  61.3 2.9 %fusion.49 = f32[32,4,8,128]{3,2,1,0:T(8,128)S(1)} fusion(bf16[2048,512]{1,0:T(8,128)(2,1)} %param.24, f32[512]{0:T(512)S(1)} %copy-done.19, bf16[256,2048]{1,0:T(8,128)(2,1)} %all-gather.6.cloned.1.call-done, f32[2048]{0:T(1024)S(1)} %convert_element_type.95, f32[256]{0:T(256)S(1)} %add_rsqrt_fusion.2), kind=kOutput, calls=%fused_computation.67 | convolution fusion | flops 539361280 | bytes 3681280 | tf_op jit(solution)/shard_map/dot_general | solution.py:117
  70.2 72.7 %while.26 = (s32[]{:T(128)}, f32[4,128,128]{2,1,0:T(8,128)S(1)}, f32[4,4,64,128]{3,2,0,1:T(8,128)}, f32[4,4,64,128]{3,2,0,1:T(8,128)}, f32[4,4,64,128]{3,2,0,1:T...) while((s32[]{:T(128)}, f32[4,128,128]{2,1,0:T(8,128)S(1)}, ...), condition=%wide.region_3.4_spmd.clone, body=%wide.region_1.3_spmd.clone.sunk | while | flops 138760192 | bytes 20862112 | solution.py:71
  75.4 7.3 %fusion.101 = f32[4,64,64]{1,2,0:T(8,128)S(1)} fusion(f32[4,64,64,128]{3,2,1,0:T(8,128)S(1)} %select_exponential_fusion.2, f32[4,128,64]{1,2,0:T(8,128)S(1)} %copy-done.1, f32[4,128,64]{1,2,0:T(8,128)S(1)} %dynamic-slice_bitcast_fusion.6), kind=kLoop, calls=%fused_computation.7.clone.1 | loop fusion | flops 6275072 | bytes 8716288 | tf_op jit(solution)/shard_map/while/body/eval_jaxpr/hid,hjd,hijd->hij/dot_general | solution.py:53
  82.7 2.0 fusion.102
  84.7 2.0 fusion.103
  93.6 7.3 %fusion.101 = f32[4,64,64]{1,2,0:T(8,128)S(1)} fusion(f32[4,64,64,128]{3,2,1,0:T(8,128)S(1)} %select_exponential_fusion.2, f32[4,128,64]{1,2,0:T(8,128)S(1)} %copy-done.1, f32[4,128,64]{1,2,0:T(8,128)S(1)} %dynamic-slice_bitcast_fusion.6), kind=kLoop, calls=%fused_computation.7.clone.1 | loop fusion | flops 6275072 | bytes 8716288 | tf_op jit(solution)/shard_map/while/body/eval_jaxpr/hid,hjd,hijd->hij/dot_general | solution.py:53
  102.9 2.0 fusion.103
  111.8 7.3 %fusion.101 = f32[4,64,64]{1,2,0:T(8,128)S(1)} fusion(f32[4,64,64,128]{3,2,1,0:T(8,128)S(1)} %select_exponential_fusion.2, f32[4,128,64]{1,2,0:T(8,128)S(1)} %copy-done.1, f32[4,128,64]{1,2,0:T(8,128)S(1)} %dynamic-slice_bitcast_fusion.6), kind=kLoop, calls=%fused_computation.7.clone.1 | loop fusion | flops 6275072 | bytes 8716288 | tf_op jit(solution)/shard_map/while/body/eval_jaxpr/hid,hjd,hijd->hij/dot_general | solution.py:53
  119.1 2.0 fusion.102
  121.1 2.0 fusion.103
  129.9 7.3 %fusion.101 = f32[4,64,64]{1,2,0:T(8,128)S(1)} fusion(f32[4,64,64,128]{3,2,1,0:T(8,128)S(1)} %select_exponential_fusion.2, f32[4,128,64]{1,2,0:T(8,128)S(1)} %copy-done.1, f32[4,128,64]{1,2,0:T(8,128)S(1)} %dynamic-slice_bitcast_fusion.6), kind=kLoop, calls=%fused_computation.7.clone.1 | loop fusion | flops 6275072 | bytes 8716288 | tf_op jit(solution)/shard_map/while/body/eval_jaxpr/hid,hjd,hijd->hij/dot_general | solution.py:53
  137.3 2.0 fusion.102
  139.2 2.0 fusion.103
  143.9 5.6 %fusion.27 = f32[8,96,768]{2,1,0:T(8,128)S(1)} fusion(bf16[1,2048,768]{2,1,0:T(8,128)(2,1)} %param.35, bf16[8,1,96,2048]{3,2,0,1:T(8,128)(2,1)} %all-gather.8.cloned.1.call-done), kind=kOutput, calls=%fused_computation.43 | convolution fusion | flops 2415919104 | bytes 8650752 | tf_op jit(solution)/shard_map/secd,edf->secf/dot_general | solution.py:168
  149.5 2.8 %fusion.35 = bf16[8,1,96,768]{3,2,0,1:T(8,128)(2,1)S(1)} fusion(f32[8,96,768]{2,1,0:T(8,128)S(1)} %fusion.27, bf16[1,2048,768]{2,1,0:T(8,128)(2,1)S(1)} %copy-done.15, bf16[8,1,96,2048]{3,2,0,1:T(8,128)(2,1)S(1)} %copy-done.16), kind=kOutput, calls=%fused_computation.53 | convolution fusion | flops 2419458048 | bytes 9830400 | tf_op jit(solution)/shard_map/secd,edf->secf/dot_general | solution.py:169
  152.3 4.0 %fusion.31 = bf16[2048,768]{0,1:T(8,128)(2,1)} fusion(bf16[768,768]{1,0:T(8,128)(2,1)S(1)} %bitcast.253, bf16[1,768,2048]{2,1,0:T(8,128)(2,1)S(1)} %copy-done), kind=kOutput, calls=%fused_computation.47 | convolution fusion | flops 2417491968 | bytes 7471104 | tf_op jit(solution)/shard_map/secf,efo->osec/dot_general | solution.py:172
  157.0 3.6 %divide_multiply_fusion = f32[256,512]{1,0:T(8,128)} fusion(bf16[2048,512]{1,0:T(8,128)(2,1)} %param.26, bf16[256,2048]{1,0:T(8,128)(2,1)} %all-gather.6.cloned.1.call-done, f32[2048]{0:T(1024)S(1)} %copy-done.12, f32[256]{0:T(256)S(1)} %add_rsqrt_fusion.2), kind=kOutput, calls=%fused_computation.87 | convolution fusion | flops 539492352 | bytes 3679232 | tf_op jit(solution)/shard_map/dot_general | solution.py:119
  160.6 2.0 copy.121
  162.6 2.1 copy.103
  169.3 12.8 %all-gather = bf16[32,1,128]{2,1,0:T(2,128)(2,1)S(1)} all-gather(bf16[4,1,128]{2,1,0:T(2,128)(2,1)S(1)} %fusion.62), channel_id=2, replica_groups=mesh['ep'=8,'tp'=4] {'ep'}, dimensions={0}, use_global_device_ids=true | all-gather | bytes 9216 | tf_op jit(solution)/shard_map/all_gather | solution.py:16
  182.2 2.3 multiply_reduce_fusion.1
  186.3 23.3 %reduce-scatter.5.cloned.1.call-done = bf16[512,768]{0,1:T(8,128)(2,1)} async-done(((bf16[2048,768]{0,1:T(8,128)(2,1)}), bf16[512,768]{0,1:T(8,128)(2,1)}) %reduce-scatter.5.cloned.1.call-update) | async-done | bytes 786448 | tf_op jit(solution)/shard_map/reduce_scatter | solution.py:173
  209.6 4.6 %all-to-all-start.1 = ((bf16[512,8,96]{0,2,1:T(8,128)(2,1)}), bf16[512,8,96]{0,2,1:T(8,128)(2,1)}, u32[]{:S(2)}, u32[]{:S(2)}) async-start(bf16[512,8,96]{0,2,1:T(8,128)(2,1)} %bitcast.242), calls=%async_computation.3 | async-start | bytes 1572864 | tf_op jit(solution)/shard_map/all_to_all | solution.py:180
  214.8 20.4 %all-to-all-done.1 = bf16[512,8,96]{0,2,1:T(8,128)(2,1)} async-done(((bf16[512,8,96]{0,2,1:T(8,128)(2,1)}), bf16[512,8,96]{0,2,1:T(8,128)(2,1)}, u32[]{:S(2)}, u32[]{:S(2)}) %all-to-all-start.1) | async-done | bytes 786464 | tf_op jit(solution)/shard_map/all_to_all | solution.py:180
  235.2 3.9 %gather_fusion.1 = bf16[512,512]{1,0:T(8,128)(2,1)} fusion(bf16[512,768]{0,1:T(8,128)(2,1)} %bitcast.53, s32[1024]{0:T(1024)S(1)} %pad_clamp_fusion), kind=kCustom, calls=%fused_computation.1 | custom fusion | bytes 1050624 | tf_op jit(solution)/shard_map/jit(_take)/gather | solution.py:181
  239.1 2.1 gather.11
  241.2 3.9 %multiply_reduce_fusion = bf16[512,256]{0,1:T(8,128)(2,1)} fusion(bf16[512,256,2]{0,2,1:T(2,128)(2,1)} %gather.11, pred[256,2]{1,0:T(8,128)(4,1)S(1)} %copy.108, f32[256,2]{1,0:T(8,128)S(1)} %copy.112), kind=kLoop, calls=%fused_computation.69 | loop fusion | flops 917504 | bytes 788992 | tf_op jit(solution)/shard_map/reduce_sum | solution.py:183
  (147 shorter events, 54.7 us)
Async XLA Ops:
  7.2 145.1 %copy-start = (bf16[1,768,2048]{2,1,0:T(8,128)(2,1)S(1)}, bf16[1,768,2048]{2,1,0:T(8,128)(2,1)}, u32[]{:S(2)}) copy-start(bf16[1,768,2048]{2,1,0:T(8,128)(2,1)} %param.37) | copy-start | bytes 9437188
  7.2 52.5 %all-gather.6.cloned.1.call-start = ((), (), s32[]{:S(2)}) async-start(), calls=%async_computation.4 | async-start | bytes 1310720 | tf_op jit(solution)/shard_map/all_gather | solution.py:103
  30.2 8.4 %copy-start.14 = (bf16[2048]{0:T(1024)(128)(2,1)S(1)}, bf16[2048]{0:T(1024)(128)(2,1)}, u32[]{:S(2)}) copy-start(bf16[2048]{0:T(1024)(128)(2,1)} %param.22) | copy-start | bytes 12292
  33.5 27.7 %copy-start.19 = (f32[512]{0:T(512)S(1)}, f32[512]{0:T(512)}, u32[]{:S(2)}) copy-start(f32[512]{0:T(512)} %param.27) | copy-start | bytes 6148
  33.5 26.1 %all-to-all-start = ((bf16[8,1,96,512]{3,2,1,0:T(8,128)(2,1)}), bf16[8,1,96,512]{3,2,1,0:T(8,128)(2,1)}, u32[]{:S(2)}, u32[]{:S(2)}) async-start(bf16[8,1,96,512]{3,2,1,0:T(8,128)(2,1)} %bitcast.234), calls=%async_computation.1 | async-start | bytes 1572864 | tf_op jit(solution)/shard_map/all_to_all | solution.py:166
  38.6 105.3 %all-gather.8.cloned.1.call-start = ((), (), s32[]{:S(2)}) async-start(), calls=%async_computation.6 | async-start | bytes 3932160 | tf_op jit(solution)/shard_map/all_gather | solution.py:167
  38.6 29.0 %copy-start.11 = (f32[2048]{0:T(1024)}, f32[2048]{0:T(1024)S(1)}, u32[]{:S(2)}) copy-start(f32[2048]{0:T(1024)S(1)} %convert_element_type.95) | copy-start | bytes 24580
  59.6 122.5 %all-gather.10.cloned.1.call-start = ((), (), s32[]{:S(2)}) async-start(), calls=%async_computation.8 | async-start | bytes 1179648 | tf_op jit(solution)/shard_map/all_gather | solution.py:16
  61.2 3.8 %copy-start.10 = (f32[4,256]{1,0:T(4,128)S(1)}, f32[4,256]{1,0:T(4,128)}, u32[]{:S(2)}) copy-start(f32[4,256]{1,0:T(4,128)} %param.28) | copy-start | bytes 12292
  61.2 4.8 %copy-start.17 = (bf16[2048,512]{1,0:T(8,128)(2,1)S(1)}, bf16[2048,512]{1,0:T(8,128)(2,1)}, u32[]{:S(2)}) copy-start(bf16[2048,512]{1,0:T(8,128)(2,1)} %param.25) | copy-start | bytes 6291460
  64.2 2.6 %copy-start.2 = (f32[32,4,8,128]{3,2,1,0:T(8,128)}, f32[32,4,8,128]{3,2,1,0:T(8,128)S(1)}, u32[]{:S(2)}) copy-start(f32[32,4,8,128]{3,2,1,0:T(8,128)S(1)} %fusion.49) | copy-start | bytes 1572868
  64.2 1.9 copy-start.8
  66.1 1.7 copy-start.18
  68.6 0.8 copy-start.7
  73.0 2.5 copy-start.1
  91.1 2.5 copy-start.1
  109.3 2.5 copy-start.1
  127.5 2.5 copy-start.1
  143.6 66.0 %reduce-scatter.5.cloned.1.call-start = ((), (), s32[]{:S(2)}) async-start(), calls=%async_computation.7 | async-start | bytes 3932160 | tf_op jit(solution)/shard_map/reduce_scatter | solution.py:173
  143.9 5.6 %copy-start.15 = (bf16[1,2048,768]{2,1,0:T(8,128)(2,1)S(1)}, bf16[1,2048,768]{2,1,0:T(8,128)(2,1)}, u32[]{:S(2)}) copy-start(bf16[1,2048,768]{2,1,0:T(8,128)(2,1)} %param.36) | copy-start | bytes 9437188
  143.9 5.6 %copy-start.16 = (bf16[8,1,96,2048]{3,2,0,1:T(8,128)(2,1)S(1)}, bf16[8,1,96,2048]{3,2,0,1:T(8,128)(2,1)}, u32[]{:S(2)}) copy-start(bf16[8,1,96,2048]{3,2,0,1:T(8,128)(2,1)} %all-gather.8.cloned.1.call-done) | copy-start | bytes 9437188
  156.3 0.7 copy-start.20
  156.3 0.7 copy-start.12
  156.3 88.7 %reduce-scatter.3.cloned.1.call-start = ((), (), s32[]{:S(2)}) async-start(), calls=%async_computation.5 | async-start | bytes 1310720 | tf_op jit(solution)/shard_map/reduce_scatter | solution.py:140
  166.4 0.8 copy-start.3
  168.5 0.8 copy-start.4
  182.1 2.3 copy-start.5
  182.1 2.4 copy-start.6
  186.3 28.1 %copy-start.9 = (s32[256,2]{0,1:T(2,128)S(1)}, s32[256,2]{0,1:T(2,128)}, u32[]{:S(2)}) copy-start(s32[256,2]{0,1:T(2,128)} %param.33) | copy-start | bytes 6148
  186.3 28.3 %copy-start.13 = (f32[256,2]{0,1:T(2,128)S(1)}, f32[256,2]{0,1:T(2,128)}, u32[]{:S(2)}) copy-start(f32[256,2]{0,1:T(2,128)} %param.34) | copy-start | bytes 6148
  209.6 25.6 %all-to-all-start.1 = ((bf16[512,8,96]{0,2,1:T(8,128)(2,1)}), bf16[512,8,96]{0,2,1:T(8,128)(2,1)}, u32[]{:S(2)}, u32[]{:S(2)}) async-start(bf16[512,8,96]{0,2,1:T(8,128)(2,1)} %bitcast.242), calls=%async_computation.3 | async-start | bytes 1572864 | tf_op jit(solution)/shard_map/all_to_all | solution.py:180
Sparse Core Ops, SparseCore 0:
  9.8 29.0 all-gather.5
  59.7 40.7 all-gather.7
  143.7 19.4 all-gather.9
  166.1 43.5 reduce-scatter.4
  212.9 27.9 reduce-scatter.2
where the time goes:
time: 253 us; the launch traced here: 252 us
  waiting for transfers between devices  65.4 us (26%)
  other arithmetic  55.5 us (22%)
  matrix products  46.8 us (18%)
  local copies, waits for them, and re-layouts  35.2 us (14%)
  blocking collectives  24.2 us (10%)
  between operations  14.2 us (6%)
  starting transfers between devices  10 us (4%)
    dot_general x4, other arithmetic, advance(): jnp.einsum('hid,hjd,hijd->hij', query_block, key_block, decay, precision=...  29.3 us
    reduce_scatter x1, waiting for transfers between devices, per_device(): lax.psum_scatter(product.reshape(col_width * lax.axis_size('tp'), -1).ast...  23.3 us
    all_to_all x1, waiting for transfers between devices, per_device(): lax.all_to_all(slots, 'ep', split_axis=0, concat_axis=0, tiled=True)  21 us
    all_to_all x1, waiting for transfers between devices, per_device(): lax.all_to_all(outgoing, 'ep', split_axis=1, concat_axis=1, tiled=True)  20.4 us
    all_gather x1, blocking collectives, entering(): lax.all_gather(a.astype(kind), axis)  12.8 us
    psum x1, blocking collectives, per_device(): squares = lax.psum(jnp.sum(moe_values * moe_values, axis=1), 'tp')  11.4 us
    squeeze x8, local copies, waits for them, and re-layouts, block_recurrence(): lax.scan(advance, state, (split(query_rows), split(key_in), split(value),...  10.5 us
    dot_general x4, matrix products, advance(): jnp.einsum('hid,hde->hie', query_block * jnp.exp(running_state), carry, p...  7.99 us
  transfers between devices with their start and end apart: 7, of which 3 were waited for; matrix products, arithmetic and copies ran while one was open for 53% of the time, Pallas kernels for 0%

commit v1 on v0

v1 whole, which is shorter than its diff:
```python
import functools

import jax
import jax.numpy as jnp
from jax import lax
from jax.experimental import pallas as pl
from jax.experimental.pallas import tpu as pltpu
from jax.sharding import PartitionSpec as P

BLOCK = 64
epsilon = 1e-06
F32 = jnp.float32
BF16 = jnp.bfloat16
VMEM = pl.BlockSpec(memory_space=pltpu.VMEM)
LIMIT = 60 * 1024 * 1024


def dot(a, b, dims=((1,), (0,)), precision=None):
    return lax.dot_general(a, b, (dims, ((), ())), precision=precision, preferred_element_type=F32)


def sigmoid(x):
    return 1.0 / (1.0 + jnp.exp(-x))


def iota(shape, dim):
    return lax.broadcasted_iota(jnp.int32, shape, dim)


def mixer_kernel(per, x_ref, gain_ref, wq_ref, wf_ref, wi_ref, wo_ref, gap_ref, dec_ref,
                 lo_ref, qd_ref, og_ref, st_ref, normed):
    step = pl.program_id(0)
    length = normed.shape[0]
    dim = st_ref.shape[2]
    parts, _, cols = x_ref.shape

    @pl.when(step == 0)
    def _():
        total = jnp.zeros((length, 1), F32)
        for p in range(parts):
            v = x_ref[p].astype(F32)
            total += jnp.sum(v * v, axis=1, keepdims=True)
        scale = lax.rsqrt(total / (parts * cols) + epsilon)
        for p in range(parts):
            g = gain_ref[:, p * cols:(p + 1) * cols].astype(F32)
            normed[:, p * cols:(p + 1) * cols] = (x_ref[p].astype(F32) * scale * g).astype(BF16)

    n = normed[...]
    qp = dot(n, wq_ref[...])
    fp = dot(n, wf_ref[...])
    value = dot(n, wi_ref[...]).astype(BF16)
    op = dot(n, wo_ref[...])
    query = qp * sigmoid(qp)
    key = gap_ref[...] * sigmoid(-fp)
    og_ref[...] = op * sigmoid(op)
    logs = jnp.log1p(-key)
    dec = dec_ref[...]
    tri = (iota((length, length), 0) >= iota((length, length), 1)).astype(F32)
    causal = iota((BLOCK, BLOCK), 0) >= iota((BLOCK, BLOCK), 1)
    half = BLOCK // 2
    for j in range(per):
        c = slice(j * dim, (j + 1) * dim)
        extra = jnp.sum(jnp.where(iota(dec.shape, 1) == step * per + j, dec, 0.0), axis=1, keepdims=True)
        run = dot(tri, logs[:, c] + extra, precision=lax.Precision.HIGHEST)
        q, k, v = query[:, c], key[:, c], value[:, c]
        qd_ref[:, c] = (q * jnp.exp(run)).astype(BF16)
        state = jnp.zeros((dim, dim), F32)
        base = jnp.zeros((1, dim), F32)
        for b in range(length // BLOCK):
            r = slice(b * BLOCK, (b + 1) * BLOCK)
            g, qb, kb, vb = run[r], q[r], k[r], v[r]
            ref = g[half - 1:half]
            last = g[BLOCK - 1:BLOCK]
            qe = (qb * jnp.exp(g - ref)).astype(BF16)
            ke = (kb * jnp.exp(ref - g)).astype(BF16)
            scores = jnp.where(causal, dot(qe, ke, ((1,), (1,))), 0.0).astype(BF16)
            out = dot(scores, vb)
            if b:
                qs = (qb * jnp.exp(g - base)).astype(BF16)
                out += dot(qs, state.astype(BF16), ((1,), (1,)))
            lo_ref[r, c] = out
            kd = (kb * jnp.exp(last - g)).astype(BF16)
            state = state * jnp.exp(last - base) + dot(vb, kd, ((0,), (0,)))
            base = last
        st_ref[j, 0:dim, :] = state.astype(BF16)
        st_ref[j, dim:, :] = jnp.broadcast_to(jnp.exp(base), (st_ref.shape[1] - dim, dim)).astype(BF16)


def mixer(x, gain, wq, wf, wi, wo, gap, dec):
    parts, length, cols = x.shape
    heads, dim = dec.shape[1], wq.shape[1] // dec.shape[1]
    per = 2 if heads % 2 == 0 else 1
    width = per * dim
    depth = wq.shape[0]
    column = pl.BlockSpec((depth, width), lambda i: (0, i))
    rows = pl.BlockSpec((length, width), lambda i: (0, i))
    whole = lambda s: pl.BlockSpec(s, lambda i: (0,) * len(s))
    return pl.pallas_call(
        functools.partial(mixer_kernel, per),
        grid=(heads // per,),
        in_specs=[whole(x.shape), whole((1, depth)), column, column, column, column,
                  pl.BlockSpec((1, width), lambda i: (0, i)), whole(dec.shape)],
        out_specs=[rows, rows, rows, pl.BlockSpec((per, dim + 16, dim), lambda i: (i, 0, 0))],
        out_shape=[jax.ShapeDtypeStruct((length, heads * dim), F32),
                   jax.ShapeDtypeStruct((length, heads * dim), BF16),
                   jax.ShapeDtypeStruct((length, heads * dim), F32),
                   jax.ShapeDtypeStruct((heads, dim + 16, dim), BF16)],
        scratch_shapes=[pltpu.VMEM((length, depth), BF16)],
        compiler_params=pltpu.CompilerParams(vmem_limit_bytes=LIMIT),
        cost_estimate=pl.CostEstimate(flops=10 * 10**9, bytes_accessed=9 * 10**6, transcendentals=10**6),
    )(x, gain.reshape(1, -1), wq, wf, wi, wo, gap.reshape(1, -1), dec)


def tail_kernel(states_ref, lo_ref, qd_ref, og_ref, hg_ref, w_ref, out_ref, gated):
    place = lax.axis_index("ep")
    hops, heads, _, dim = states_ref.shape
    for h in range(heads):
        c = slice(h * dim, (h + 1) * dim)

        def one(hop, state):
            own = states_ref[hop, h, 0:dim, :].astype(F32)
            passing = states_ref[hop, h, dim:dim + 16, :].astype(F32)[0:1]
            return jnp.where(hop < place, state * passing + own, state)

        state = lax.fori_loop(0, hops, one, jnp.zeros((dim, dim), F32))
        out = lo_ref[:, c] + dot(qd_ref[:, c], state.astype(BF16), ((1,), (1,)))
        scale = lax.rsqrt(jnp.mean(out * out, axis=1, keepdims=True) + epsilon)
        gated[:, c] = (out * scale * hg_ref[...].astype(F32) * og_ref[:, c]).astype(BF16)
    parts, _, cols = out_ref.shape
    for p in range(parts):
        out_ref[p] = dot(gated[...], w_ref[:, p * cols:(p + 1) * cols]).astype(BF16)


def tail(states, lo, qd, og, hg, w, parts):
    length, width = lo.shape
    return pl.pallas_call(
        tail_kernel,
        in_specs=[VMEM] * 6,
        out_specs=VMEM,
        out_shape=jax.ShapeDtypeStruct((parts, length, w.shape[1] // parts), BF16),
        scratch_shapes=[pltpu.VMEM((length, width), BF16)],
        compiler_params=pltpu.CompilerParams(vmem_limit_bytes=LIMIT),
        cost_estimate=pl.CostEstimate(flops=10**9, bytes_accessed=5 * 10**6, transcendentals=10**5),
    )(states, lo, qd, og, hg.reshape(1, -1), w)


def ranks(ids, experts):
    tokens = ids.shape[1]
    names = iota((experts, tokens), 0)
    picks = [names == ids[k:k + 1, :] for k in range(ids.shape[0])]
    chosen = functools.reduce(jnp.logical_or, picks)
    before = (iota((tokens, tokens), 0) < iota((tokens, tokens), 1)).astype(BF16)
    return picks, chosen, dot(chosen.astype(BF16), before)


def slot_hits(mask, rank, experts, capacity):
    rows = experts * capacity
    owner = iota((rows, experts), 0) - iota((rows, experts), 1) * capacity
    owner = jnp.logical_and(owner >= 0, owner < capacity).astype(F32)
    tokens = rank.shape[1]
    spread = dot(owner, jnp.where(mask, rank, -1.0))
    spot = dot(owner, iota((experts, tokens), 0).astype(F32)) * capacity
    return (spread >= 0.0) & (spread + spot == iota((rows, tokens), 0).astype(F32))


def dispatch_kernel(experts, capacity, ids_ref, rows_ref, out_ref):
    _, chosen, rank = ranks(ids_ref[...], experts)
    hits = slot_hits(chosen, rank, experts, capacity).astype(BF16)
    out_ref[...] = dot(hits, rows_ref[...]).astype(BF16)


def dispatch(ids, rows, experts, capacity):
    return pl.pallas_call(
        functools.partial(dispatch_kernel, experts, capacity),
        in_specs=[VMEM] * 2,
        out_specs=VMEM,
        out_shape=jax.ShapeDtypeStruct((experts * capacity, rows.shape[1]), BF16),
    )(ids, rows)


def combine_kernel(experts, capacity, ids_ref, scores_ref, back_ref, out_ref):
    picks, _, rank = ranks(ids_ref[...], experts)
    scores = scores_ref[...]
    weights = scores / jnp.sum(scores, axis=1, keepdims=True)
    total = jnp.zeros(out_ref.shape, F32)
    for k, mask in enumerate(picks):
        hits = slot_hits(mask, rank, experts, capacity).astype(BF16)
        total += dot(hits, back_ref[...], ((0,), (0,))) * weights[:, k:k + 1]
    out_ref[...] = total.astype(BF16)


def combine(ids, scores, back, experts, capacity):
    return pl.pallas_call(
        functools.partial(combine_kernel, experts, capacity),
        in_specs=[VMEM] * 3,
        out_specs=VMEM,
        out_shape=jax.ShapeDtypeStruct((ids.shape[1], back.shape[1]), BF16),
    )(ids, scores, back)


def expert_kernel(x_ref, gain_ref, wg_ref, wu_ref, wd_ref, out_ref, normed, total):
    step = pl.program_id(0)
    parts, rows, cols = x_ref.shape

    @pl.when(step == 0)
    def _():
        squares = jnp.zeros((rows, 1), F32)
        for p in range(parts):
            v = x_ref[p].astype(F32)
            squares += jnp.sum(v * v, axis=1, keepdims=True)
        scale = lax.rsqrt(squares / (parts * cols) + epsilon)
        for p in range(parts):
            g = gain_ref[:, p * cols:(p + 1) * cols].astype(F32)
            normed[:, p * cols:(p + 1) * cols] = (x_ref[p].astype(F32) * scale * g).astype(BF16)

    gate = dot(normed[...], wg_ref[0])
    up = dot(normed[...], wu_ref[0])
    hidden = (gate * sigmoid(gate) * up).astype(BF16)
    last = pl.num_programs(0) - 1
    for p in range(parts):
        c = slice(p * cols, (p + 1) * cols)
        part = dot(hidden, wd_ref[0, :, c])

        @pl.when(jnp.logical_and(step == 0, last > 0))
        def _():
            total[:, c] = part

        @pl.when(jnp.logical_and(step > 0, step < last))
        def _():
            total[:, c] += part

        @pl.when(step == last)
        def _():
            out_ref[p] = (jnp.where(step > 0, total[:, c], 0.0) + part).astype(BF16)


def experts_call(x, gain, wg, wu, wd):
    parts, rows, cols = x.shape
    depth, units = wg.shape[1:]
    tile = 256 if units % 256 == 0 else units
    return pl.pallas_call(
        expert_kernel,
        grid=(units // tile,),
        in_specs=[pl.BlockSpec(x.shape, lambda i: (0, 0, 0)), pl.BlockSpec((1, depth), lambda i: (0, 0)),
                  pl.BlockSpec((1, depth, tile), lambda i: (0, 0, i)),
                  pl.BlockSpec((1, depth, tile), lambda i: (0, 0, i)),
                  pl.BlockSpec((1, tile, depth), lambda i: (0, i, 0))],
        out_specs=pl.BlockSpec(x.shape, lambda i: (0, 0, 0)),
        out_shape=jax.ShapeDtypeStruct(x.shape, BF16),
        scratch_shapes=[pltpu.VMEM((rows, depth), BF16), pltpu.VMEM((rows, depth), F32)],
        compiler_params=pltpu.CompilerParams(vmem_limit_bytes=LIMIT),
        cost_estimate=pl.CostEstimate(flops=8 * 10**9, bytes_accessed=10**7, transcendentals=10**6),
    )(x, gain.reshape(1, -1), wg, wu, wd)


def per_device(mix_rows, mix_gain, w_query, w_forget, w_input, w_outgate, forget_gap, decay_extra,
               head_gain, w_mixout, moe_rows, moe_gain, route_ids, route_scores, w_gate, w_up, w_down):
    eps, tps = lax.axis_size("ep"), lax.axis_size("tp")
    tokens, top = route_ids.shape
    experts = w_gate.shape[0] * eps
    capacity = tokens * top * 3 // (2 * experts)
    cols = mix_rows.shape[1]
    ids = route_ids.T
    slots = dispatch(ids, moe_rows, experts, capacity)
    arrived = lax.all_to_all(slots.reshape(eps, -1, cols), "ep", split_axis=0, concat_axis=0, tiled=True)
    gathered = lax.all_gather(arrived.reshape(-1, cols), "tp", axis=0)
    mix_whole = lax.all_gather(mix_rows, "tp", axis=0)
    lo, qd, og, st = mixer(mix_whole, mix_gain, w_query, w_forget, w_input, w_outgate, forget_gap, decay_extra.T)
    product = experts_call(gathered, moe_gain, w_gate, w_up, w_down)
    expert_sum = lax.psum_scatter(product, "tp", scatter_dimension=0)
    states = lax.all_gather(st, "ep", axis=0)
    mixed = tail(states, lo, qd, og, head_gain, w_mixout, tps)
    mix_out = lax.psum_scatter(mixed, "tp", scatter_dimension=0)
    back = lax.all_to_all(expert_sum.reshape(eps, -1, cols), "ep", split_axis=0, concat_axis=0, tiled=True)
    moe_out = combine(ids, route_scores, back.reshape(-1, cols), experts, capacity)
    return (mix_out, moe_out)


def solution(mesh):
    placed = (
        P("ep", "tp"), P(), P(None, "tp"), P(None, "tp"), P(None, "tp"), P(None, "tp"), P("tp"),
        P("tp", "ep"), P(), P("tp", None), P("ep", "tp"), P(), P("ep", None), P("ep", None),
        P("ep", None, "tp"), P("ep", None, "tp"), P("ep", "tp", None),
    )
    return jax.shard_map(
        per_device, mesh=mesh, in_specs=placed,
        out_specs=(P("ep", "tp"), P("ep", "tp")), check_vma=False,
    )
```

time: 253 us -> 195 us (0.77)
  other arithmetic: 55.5 us -> 0 us
  matrix products: 46.8 us -> 0 us
  Pallas kernels: 0 us -> 40 us
  waiting for transfers between devices: 65.4 us -> 104 us
  local copies, waits for them, and re-layouts: 35.2 us -> 3.74 us
  starting transfers between devices: 10 us -> 4.81 us
  blocking collectives: 24.2 us -> 27.4 us
    dot_general x21 -> x0, matrix products: 46.8 us -> none  [the longest x4 7.99 us: advance(): jnp.einsum('hid,hde->hie', query_block * jnp.exp(running_state), carry, p...]
    unnamed x5 -> x7, waiting for transfers between devices: 0.75 us -> 43.2 us
    all_gather x3, waiting for transfers between devices: 0.04 us -> 41.1 us  [the longest x1 33.2 us: per_device(): gathered = lax.all_gather(arrived.reshape(-1, cols), 'tp', axis=0)]
    pallas_call x0 -> x5, Pallas kernels: none -> 40 us  [the longest x1 17 us: experts_call(): pl.pallas_call(expert_kernel, grid=(units // tile,), in_specs=[pl.BlockSp...]
    dot_general x4 -> x0, other arithmetic: 29.3 us -> none  [advance(): jnp.einsum('hid,hjd,hijd->hij', query_block, key_block, decay, precision=...]
    all_to_all x0 -> x1, blocking collectives: none -> 27.4 us  [per_device(): lax.all_to_all(slots.reshape(eps, -1, cols), 'ep', split_axis=0, concat_a...]
    reduce_scatter x2 -> x0, waiting for transfers between devices: 23.3 us -> none  [the longest x1 23.3 us: per_device(): lax.psum_scatter(product.reshape(col_width * lax.axis_size('tp'), -1).ast...]
    all_to_all x2 -> x1, waiting for transfers between devices: 41.4 us -> 20.1 us  [per_device(): lax.all_to_all(expert_sum.reshape(eps, -1, cols), 'ep', split_axis=0, con...]
  transfers between devices with their start and end apart: 7 -> 6, of which waited for: 3 -> 5; matrix products, arithmetic and copies ran while one was open for 53% -> 1% of each run, Pallas kernels for 0% -> 21%
where the time goes in v1:
time: 195 us; the launch traced here: 194 us
  waiting for transfers between devices  104 us (53%)
  Pallas kernels  40 us (21%)
  blocking collectives  27.4 us (14%)
  between operations  13.8 us (7%)
  starting transfers between devices  4.81 us (2%)
  local copies, waits for them, and re-layouts  3.74 us (2%)
    unnamed x7, waiting for transfers between devices  43.2 us
    all_gather x1, waiting for transfers between devices, per_device(): gathered = lax.all_gather(arrived.reshape(-1, cols), 'tp', axis=0)  33.2 us
    all_to_all x1, blocking collectives, per_device(): lax.all_to_all(slots.reshape(eps, -1, cols), 'ep', split_axis=0, concat_a...  27.4 us
    all_to_all x1, waiting for transfers between devices, per_device(): lax.all_to_all(expert_sum.reshape(eps, -1, cols), 'ep', split_axis=0, con...  20.1 us
    pallas_call x1, Pallas kernels, experts_call(): pl.pallas_call(expert_kernel, grid=(units // tile,), in_specs=[pl.BlockSp...  17 us
    pallas_call x1, Pallas kernels, mixer(): pl.pallas_call(functools.partial(mixer_kernel, per), grid=(heads // per,)...  11.6 us
    all_gather x1, waiting for transfers between devices, per_device(): states = lax.all_gather(st, 'ep', axis=0)  7.91 us
    pallas_call x1, Pallas kernels, tail(): pl.pallas_call(tail_kernel, in_specs=[VMEM] * 6, out_specs=VMEM, out_shap...  5.45 us
  transfers between devices with their start and end apart: 6, of which 5 were waited for; matrix products, arithmetic and copies ran while one was open for 1% of the time, Pallas kernels for 21%

profile of v1, /device:TPU:0, one launch (start us, length us, event | category | flops | bytes accessed | tf_op | source)
XLA Modules:
  0.0 194.2 jit_solution(4513498699415049200)
XLA Ops:
  7.2 0.0 copy-start.1
  7.2 0.0 copy-start.2
  7.2 0.0 all-gather.8.cloned.1.call-start
  7.2 0.7 all-gather.8.cloned.1.call-update
  7.9 0.0 all-gather.6.cloned.1.call-start
  8.0 2.6 %shard_map.178 = bf16[768,512]{1,0:T(8,128)(2,1)} custom-call(s32[2,256]{1,0:T(2,128)} %bitcast.18, bf16[256,512]{1,0:T(8,128)(2,1)} %rows_ref.1), custom_call_target="tpu_custom_call" | custom-call | tf_op jit(solution)/shard_map/pallas_call | solution.py:173
  10.5 27.4 %all_to_all.10 = bf16[8,96,512]{2,1,0:T(8,128)(2,1)} all-to-all(bf16[8,96,512]{2,1,0:T(8,128)(2,1)} %bitcast.14), channel_id=1, replica_groups=mesh['ep'=8,'tp'=4] {'ep'}, dimensions={0} | all-to-all | bytes 1572864 | tf_op jit(solution)/shard_map/all_to_all | solution.py:265
  37.9 0.0 all-gather.6.cloned.1.call-update
  38.0 0.0 all-gather.10.cloned.1.call-start
  38.0 0.0 copy-done.1
  38.0 0.8 copy.21
  38.8 0.6 reshape.22.gain_ref
  39.4 11.6 %shard_map.176 = (f32[256,512]{1,0:T(8,128)}, bf16[256,512]{1,0:T(8,128)(2,1)}, f32[256,512]{1,0:T(8,128)}, bf16[4,144,128]{2,1,0:T(8,128)(2,1)}) custom-call(bf16[4,256,512]{2,1,0:T(8,128)(2,1)} %bitcast.21, bf16[1,2048]{1,0:T(2,128)(2,1)} %reshape.22.gain_ref, bf16[2048,512]{1,0:T(8,128)(2,1)} %wq_ref.1, bf16[2048,512]{1,0:T(8,128)(2,1)} %wf_ref.1, ...), custom_call_target="tpu_custom_call" | custom-call | flops 10000000000 | bytes 9000000 | tf_op jit(solution)/shard_map/pallas_call | solution.py:98
  51.0 0.0 all-gather.10.cloned.1.call-update
  51.1 0.0 reduce-scatter.9.cloned.1.call-start
  51.1 0.0 copy-done.3
  51.1 0.6 reshape.26.gain_ref
  51.7 33.2 %all-gather.6.cloned.1.call-done.x_ref = bf16[4,768,512]{2,1,0:T(8,128)(2,1)} async-done(((bf16[1,768,512]{2,1,0:T(8,128)(2,1)}), bf16[4,768,512]{2,1,0:T(8,128)(2,1)}) %all-gather.6.cloned.1.call-update) | async-done | bytes 3145744 | tf_op jit(solution)/shard_map/all_gather | solution.py:266
  84.9 17.0 %shard_map.179 = bf16[4,768,512]{2,1,0:T(8,128)(2,1)} custom-call(bf16[4,768,512]{2,1,0:T(8,128)(2,1)} %all-gather.6.cloned.1.call-done.x_ref, bf16[1,2048]{1,0:T(2,128)(2,1)} %reshape.26.gain_ref, bf16[1,2048,768]{2,1,0:T(8,128)(2,1)} %wg_ref.1, bf16[1,2048,768]{2,1,0:T(8,128)(2,1)} %wu_ref.1, bf16[1,768,2048]{2,1,0:T(8,128)(2,1)} %wd_ref.1), custom_call_target="tpu_custom_call" | custom-call | flops 8000000000 | bytes 10000000 | tf_op jit(solution)/shard_map/pallas_call | solution.py:241
  102.0 0.0 reduce-scatter.9.cloned.1.call-update
  102.0 0.0 reduce-scatter.7.cloned.1.call-start
  102.1 7.9 %all-gather.10.cloned.1.call-done = bf16[32,144,128]{2,1,0:T(8,128)(2,1)} async-done(((bf16[4,144,128]{2,1,0:T(8,128)(2,1)}), bf16[32,144,128]{2,1,0:T(8,128)(2,1)}) %all-gather.10.cloned.1.call-update) | async-done | bytes 1179664 | tf_op jit(solution)/shard_map/all_gather | solution.py:271
  110.0 5.4 %shard_map.177 = bf16[4,256,512]{2,1,0:T(8,128)(2,1)} custom-call(bf16[8,4,144,128]{3,2,1,0:T(8,128)(2,1)} %bitcast.15, f32[256,512]{1,0:T(8,128)} %get-tuple-element.7.lo_ref, bf16[256,512]{1,0:T(8,128)(2,1)} %get-tuple-element.8.qd_ref, f32[256,512]{1,0:T(8,128)} %get-tuple-element.9.og_ref, bf16[1,128]{1,0:T(2,128)(2,1)} %bitcast.20, bf16[512,2048]{1,0:T(8,128)(2,1)} %w_ref.1), custom_call_target="tpu_custom_call" | custom-call | flops 1000000000 | bytes 5000000 | tf_op jit(solution)/shard_map/pallas_call | solution.py:136
  115.4 0.0 reduce-scatter.7.cloned.1.call-update
  115.4 40.9 %reduce-scatter.9.cloned.1.call-done = bf16[1,768,512]{2,1,0:T(8,128)(2,1)} async-done(((bf16[4,768,512]{2,1,0:T(8,128)(2,1)}), bf16[1,768,512]{2,1,0:T(8,128)(2,1)}) %reduce-scatter.9.cloned.1.call-update) | async-done | bytes 786448
  156.4 4.6 %all-to-all-start.1 = ((bf16[8,96,512]{2,1,0:T(8,128)(2,1)}), bf16[8,96,512]{2,1,0:T(8,128)(2,1)S(1)}, u32[]{:S(2)}, u32[]{:S(2)}) async-start(bf16[8,96,512]{2,1,0:T(8,128)(2,1)} %bitcast.16), calls=%async_computation.1 | async-start | bytes 1572864 | tf_op jit(solution)/shard_map/all_to_all | solution.py:274
  161.0 0.0 copy-done.4
  161.0 0.8 copy.22.scores_ref
  161.8 20.1 %all-to-all-done.1 = bf16[8,96,512]{2,1,0:T(8,128)(2,1)S(1)} async-done(((bf16[8,96,512]{2,1,0:T(8,128)(2,1)}), bf16[8,96,512]{2,1,0:T(8,128)(2,1)S(1)}, u32[]{:S(2)}, u32[]{:S(2)}) %all-to-all-start.1) | async-done | bytes 786464 | tf_op jit(solution)/shard_map/all_to_all | solution.py:274
  181.9 0.9 copy-done
  182.9 3.3 %shard_map.180 = bf16[256,512]{1,0:T(8,128)(2,1)} custom-call(s32[2,256]{1,0:T(2,128)} %bitcast.19, f32[256,2]{1,0:T(8,128)} %copy.22.scores_ref, bf16[768,512]{1,0:T(8,128)(2,1)} %bitcast.13), custom_call_target="tpu_custom_call" | custom-call | tf_op jit(solution)/shard_map/pallas_call | solution.py:193
  186.2 1.5 reduce-scatter.7.cloned.1.call-done
  (5 shorter events, 0.0 us)
Async XLA Ops:
  7.2 30.8 %copy-start.1 = (f32[4,256]{1,0:T(4,128)S(1)}, f32[4,256]{1,0:T(4,128)}, u32[]{:S(2)}) copy-start(f32[4,256]{1,0:T(4,128)} %param.24) | copy-start | bytes 12292
  7.2 31.6 %copy-start.2 = (bf16[2048]{0:T(1024)(128)(2,1)S(1)}, bf16[2048]{0:T(1024)(128)(2,1)}, u32[]{:S(2)}) copy-start(bf16[2048]{0:T(1024)(128)(2,1)} %param.18) | copy-start | bytes 12292
  7.2 32.2 %all-gather.8.cloned.1.call-start = ((), (), s32[]{:S(2)}) async-start(), calls=%async_computation.5 | async-start | bytes 1310720 | tf_op jit(solution)/shard_map/all_gather | solution.py:267
  7.9 77.0 %all-gather.6.cloned.1.call-start = ((), (), s32[]{:S(2)}) async-start(), calls=%async_computation.4 | async-start | bytes 3932160 | tf_op jit(solution)/shard_map/all_gather | solution.py:266
  38.0 72.0 %all-gather.10.cloned.1.call-start = ((), (), s32[]{:S(2)}) async-start(), calls=%async_computation.6 | async-start | bytes 1327104 | tf_op jit(solution)/shard_map/all_gather | solution.py:271
  39.4 11.7 %copy-start.3 = (bf16[2048]{0:T(1024)(128)(2,1)S(1)}, bf16[2048]{0:T(1024)(128)(2,1)}, u32[]{:S(2)}) copy-start(bf16[2048]{0:T(1024)(128)(2,1)} %param.28) | copy-start | bytes 12292
  51.1 105.3 %reduce-scatter.9.cloned.1.call-start = ((), (), s32[]{:S(2)}) async-start(), calls=%async_computation.8 | async-start | bytes 3932160
  102.0 85.7 %reduce-scatter.7.cloned.1.call-start = ((), (), s32[]{:S(2)}) async-start(), calls=%async_computation.7 | async-start | bytes 1310720
  115.4 45.6 %copy-start.4 = (f32[256,2]{0,1:T(2,128)S(1)}, f32[256,2]{0,1:T(2,128)}, u32[]{:S(2)}) copy-start(f32[256,2]{0,1:T(2,128)} %param.30) | copy-start | bytes 6148
  156.4 25.6 %all-to-all-start.1 = ((bf16[8,96,512]{2,1,0:T(8,128)(2,1)}), bf16[8,96,512]{2,1,0:T(8,128)(2,1)S(1)}, u32[]{:S(2)}, u32[]{:S(2)}) async-start(bf16[8,96,512]{2,1,0:T(8,128)(2,1)} %bitcast.16), calls=%async_computation.1 | async-start | bytes 1572864 | tf_op jit(solution)/shard_map/all_to_all | solution.py:274
  181.9 0.9 copy-start
Sparse Core Ops, SparseCore 0:
  9.8 29.2 all-gather.7
  40.9 43.9 all-gather.5
  87.2 22.7 all-gather.9
  112.8 43.5 reduce-scatter.8
  159.7 27.9 reduce-scatter.6
